TPU v7x, 32 devices: a whole 2x2x4 slice. The times are simulated.
32 devices in a mesh: sp: 8 (over z, y), dp: 4 (over x, core).
Axes of the slice: x: 2, y: 2, z: 4, core: 2. Of those that a mesh axis runs over, the one named last changes fastest.
Arguments:
- tokens: bfloat16 [4, 512, 1024], P('dp', 'sp'), may hold values from -6 to 6
- w_query: bfloat16 [1024, 512], P(None, ('sp', 'dp')), may hold values from -0.1875 to 0.1875
- w_forward: bfloat16 [1024, 512], P(None, ('sp', 'dp')), may hold values from -0.1875 to 0.1875
- w_backward: bfloat16 [1024, 512], P(None, ('sp', 'dp')), may hold values from -0.1875 to 0.1875
- w_input: bfloat16 [1024, 512], P(None, ('sp', 'dp')), may hold values from -0.1875 to 0.1875
- w_gate: bfloat16 [1024, 512], P(None, ('sp', 'dp')), may hold values from -0.1875 to 0.1875
- w_out: bfloat16 [512, 1024], P(None, ('sp', 'dp')), may hold values from -0.25 to 0.25
- memory_forward: float32 [512], replicated, may hold values from 0.3 to 4
- memory_backward: float32 [512], replicated, may hold values from 0.3 to 4
- norm_gain: float32 [128], replicated, may hold values from 0.1 to 1.9
Outputs:
- mixed: bfloat16 [4, 512, 1024], P('dp', 'sp')
All inputs are finite; a program needn't handle non-finite values.
Results may differ from a plain program's by a relative error of at most 0.015.
Values may be sent and summed in bfloat16 or wider, within the bound.
A program may use at most 64 MiB of HBM per device.

v0:
```python
import jax
import jax.numpy as jnp
from jax import lax
from jax.sharding import PartitionSpec as P

HEADS = 4
HEAD_DIM = 128
BLOCK = 64
norm_eps = 1e-06
highest = lax.Precision.HIGHEST


def as_sent(array):
    return jax.tree.map(lambda a: a.astype(jnp.bfloat16) if a.dtype == jnp.float32 else a, array)


def gathered_then(share, axis, dim, apply):
    everything = lax.all_gather(share, axis, axis=dim, tiled=True)
    return apply(everything, jnp.int32(0))


def log_forget(projected, memory, seq_len):
    slack_value = memory / seq_len
    return jnp.logaddexp(
        jnp.log1p(-slack_value),
        jnp.log(slack_value) + jax.nn.log_sigmoid(projected.astype(jnp.float32)),
    )


def sweep(queries, log_decay, values):
    seq_len, key_width = queries.shape
    blocks = seq_len // BLOCK
    input_keys = -jnp.expm1(log_decay)
    lower_mask = jnp.tril(jnp.ones((BLOCK, BLOCK), dtype=bool))[:, :, None]

    def advance(carry_state, inputs):
        query_part, decay_part, key_part, value_part = inputs
        running = jnp.cumsum(decay_part, axis=0)
        from_state = jnp.dot(query_part * jnp.exp(running), carry_state, precision=highest)
        gaps = running[:, None, :] - running[None, :, :]
        decay_table = jnp.where(lower_mask, jnp.exp(jnp.where(lower_mask, gaps, 0.0)), 0.0)
        scores = jnp.sum(query_part[:, None, :] * key_part[None, :, :] * decay_table, axis=2)
        inside = jnp.dot(scores, value_part, precision=highest)
        final_sum = running[-1]
        weighted = key_part * jnp.exp(final_sum[None, :] - running)
        carry_state = jnp.exp(final_sum)[:, None] * carry_state + jnp.dot(
            weighted.T, value_part, precision=highest
        )
        return (carry_state, from_state + inside)

    def blocked(array):
        return array.reshape(blocks, BLOCK, array.shape[1])

    zero_state = jnp.zeros((key_width, values.shape[1]), jnp.float32)
    _, readings = lax.scan(
        advance,
        zero_state,
        (blocked(queries), blocked(log_decay), blocked(input_keys), blocked(values)),
    )
    return readings.reshape(seq_len, values.shape[1])


def both_ways(queries, log_ahead, log_behind, values):
    forward_read = sweep(queries, log_ahead, values)
    behind = sweep(jnp.flip(queries, 0), jnp.flip(log_behind, 0), jnp.flip(values, 0))
    return forward_read + jnp.flip(behind, 0)


def body(
    tokens,
    w_query,
    w_forward,
    w_backward,
    w_input,
    w_gate,
    w_out,
    memory_forward,
    memory_backward,
    norm_gain,
):
    seq_count, tok_count, model_width = tokens.shape
    row_count = seq_count * tok_count
    flat_tokens = tokens.reshape(row_count, model_width)
    group_count = lax.axis_size("sp")
    per_head_groups = group_count // HEADS
    block_width = HEAD_DIM // per_head_groups
    head_index = lax.axis_index("sp") // per_head_groups
    full_query, full_forward, full_backward, full_input, full_gate = (
        lax.all_gather(w_query, ("sp", "dp"), axis=1, tiled=True),
        lax.all_gather(w_forward, ("sp", "dp"), axis=1, tiled=True),
        lax.all_gather(w_backward, ("sp", "dp"), axis=1, tiled=True),
        lax.all_gather(w_input, ("sp", "dp"), axis=1, tiled=True),
        lax.all_gather(w_gate, ("sp", "dp"), axis=1, tiled=True),
    )

    def project(weight):
        return jnp.dot(flat_tokens, weight, preferred_element_type=jnp.float32).astype(jnp.bfloat16)

    def by_head(projected):
        shaped = projected.reshape(row_count, HEADS, 1, HEAD_DIM)
        spread_out = jnp.broadcast_to(shaped, (row_count, HEADS, per_head_groups, HEAD_DIM))
        return spread_out.reshape(row_count, group_count, HEAD_DIM)

    def by_group(projected):
        return projected.reshape(row_count, group_count, block_width)

    query_heads, ahead_heads, behind_heads, value_heads = (
        lax.all_to_all(
            as_sent(by_head(project(full_query))), "sp", split_axis=1, concat_axis=0, tiled=True
        ),
        lax.all_to_all(
            as_sent(by_head(project(full_forward))), "sp", split_axis=1, concat_axis=0, tiled=True
        ),
        lax.all_to_all(
            as_sent(by_head(project(full_backward))), "sp", split_axis=1, concat_axis=0, tiled=True
        ),
        lax.all_to_all(
            as_sent(by_group(project(full_input))), "sp", split_axis=1, concat_axis=0, tiled=True
        ),
    )
    gate_rows = project(full_gate)
    seq_len = query_heads.shape[0]
    memory_ahead = lax.dynamic_slice_in_dim(memory_forward, head_index * HEAD_DIM, HEAD_DIM)
    memory_behind = lax.dynamic_slice_in_dim(memory_backward, head_index * HEAD_DIM, HEAD_DIM)
    queries = jax.nn.silu(query_heads[:, 0].astype(jnp.float32))
    log_ahead = log_forget(ahead_heads[:, 0], memory_ahead, seq_len)
    log_behind = log_forget(behind_heads[:, 0], memory_behind, seq_len)
    values = value_heads[:, 0].astype(jnp.float32)
    readout = both_ways(queries, log_ahead, log_behind, values).astype(jnp.bfloat16)
    returned = lax.all_to_all(
        readout.reshape(seq_len, 1, block_width), "sp", split_axis=0, concat_axis=1, tiled=True
    )
    readout_rows = returned.reshape(row_count, HEADS, HEAD_DIM).astype(jnp.float32)
    normed = (
        readout_rows
        * lax.rsqrt(jnp.mean(readout_rows * readout_rows, axis=-1, keepdims=True) + norm_eps)
        * norm_gain
    )
    normed = normed.reshape(row_count, HEADS * HEAD_DIM)
    gated_rows = (normed * jax.nn.silu(gate_rows.astype(jnp.float32))).astype(jnp.bfloat16)

    def output_block(weight_piece, first_index):
        return jnp.dot(gated_rows, weight_piece, preferred_element_type=jnp.float32).astype(
            jnp.bfloat16
        )

    mixed_rows = gathered_then(w_out, ("sp", "dp"), 1, output_block)
    return mixed_rows.reshape(seq_count, tok_count, model_width)


def solution(mesh):
    return jax.shard_map(
        body,
        mesh=mesh,
        in_specs=(
            P("dp", "sp", None),
            P(None, ("sp", "dp")),
            P(None, ("sp", "dp")),
            P(None, ("sp", "dp")),
            P(None, ("sp", "dp")),
            P(None, ("sp", "dp")),
            P(None, ("sp", "dp")),
            P(),
            P(),
            P(),
        ),
        out_specs=P("dp", "sp", None),
        check_vma=False,
    )
```

profile of v0, /device:TPU:0, one launch (start us, length us, event | category | flops | bytes accessed | tf_op | source)
XLA Modules:
  0.0 354.7 jit_solution(13744162278260831660)
XLA Ops:
  6.5 0.7 all-gather.13.cloned.1.call-update
  7.3 0.7 all-gather.9.cloned.1.call-update
  8.1 0.7 all-gather.11.cloned.1.call-update
  9.4 0.5 all-gather.15.cloned.1.call-update
  10.5 0.8 negate_log-plus-one_fusion
  11.3 0.8 negate_log-plus-one_fusion.1
  12.1 54.5 %all-gather.13.cloned.1.call-done = bf16[1024,512]{0,1:T(8,128)(2,1)} async-done(((bf16[1024,16]{0,1:T(8,128)(2,1)}), bf16[1024,512]{0,1:T(8,128)(2,1)}) %all-gather.13.cloned.1.call-update) | async-done | bytes 1048592 | tf_op jit(solution)/shard_map/all_gather | solution.py:91
  66.6 1.7 fusion.54
  68.2 53.8 %all-gather.9.cloned.1.call-done = bf16[1024,512]{0,1:T(8,128)(2,1)} async-done(((bf16[1024,16]{0,1:T(8,128)(2,1)}), bf16[1024,512]{0,1:T(8,128)(2,1)}) %all-gather.9.cloned.1.call-update) | async-done | bytes 1048592 | tf_op jit(solution)/shard_map/all_gather | solution.py:92
  122.0 1.7 convolution_convert_fusion.4
  123.9 0.8 reshape.264
  124.7 4.5 %all-to-all-start.1 = ((bf16[8,2,2048]{2,1,0:T(2,128)(2,1)}), bf16[8,2,2048]{2,1,0:T(2,128)(2,1)S(1)}, u32[]{:S(2)}, u32[]{:S(2)}) async-start(bf16[8,2,2048]{2,1,0:T(2,128)(2,1)} %reshape.264), calls=%async_computation.1 | async-start | bytes 131072 | tf_op jit(solution)/shard_map/all_to_all | solution.py:117
  129.2 48.4 %all-gather.11.cloned.1.call-done = bf16[1024,512]{0,1:T(8,128)(2,1)} async-done(((bf16[1024,16]{0,1:T(8,128)(2,1)}), bf16[1024,512]{0,1:T(8,128)(2,1)}) %all-gather.11.cloned.1.call-update) | async-done | bytes 1048592 | tf_op jit(solution)/shard_map/all_gather | solution.py:89
  177.5 1.7 fusion.53
  179.2 53.6 %all-gather.7.cloned.1.call-done = bf16[1024,512]{0,1:T(8,128)(2,1)} async-done(((bf16[1024,16]{0,1:T(8,128)(2,1)}), bf16[1024,512]{0,1:T(8,128)(2,1)}) %all-gather.7.cloned.1.call-update) | async-done | bytes 1048592 | tf_op jit(solution)/shard_map/all_gather | solution.py:90
  232.9 1.7 fusion.52
  234.6 0.7 broadcast_in_dim.94
  235.2 4.5 %all-to-all-start.3 = ((bf16[64,8,128]{2,0,1:T(8,128)(2,1)}), bf16[64,8,128]{2,0,1:T(8,128)(2,1)S(1)}, u32[]{:S(2)}, u32[]{:S(2)}) async-start(bf16[64,8,128]{2,0,1:T(8,128)(2,1)} %bitcast.17), calls=%async_computation.3 | async-start | bytes 262144 | tf_op jit(solution)/shard_map/all_to_all | solution.py:114
  240.1 7.1 %all-to-all-done.3 = bf16[64,8,128]{2,0,1:T(8,128)(2,1)S(1)} async-done(((bf16[64,8,128]{2,0,1:T(8,128)(2,1)}), bf16[64,8,128]{2,0,1:T(8,128)(2,1)S(1)}, u32[]{:S(2)}, u32[]{:S(2)}) %all-to-all-start.3) | async-done | bytes 131104 | tf_op jit(solution)/shard_map/all_to_all | solution.py:114
  247.1 0.7 broadcast_in_dim.92
  247.8 3.4 all-to-all-start.2
  251.8 6.7 %all-to-all-done.2 = bf16[64,8,128]{2,0,1:T(8,128)(2,1)S(1)} async-done(((bf16[64,8,128]{2,0,1:T(8,128)(2,1)}), bf16[64,8,128]{2,0,1:T(8,128)(2,1)S(1)}, u32[]{:S(2)}, u32[]{:S(2)}) %all-to-all-start.2) | async-done | bytes 131104 | tf_op jit(solution)/shard_map/all_to_all | solution.py:108
  258.5 0.7 broadcast_in_dim.90
  259.1 3.4 all-to-all-start
  262.8 17.5 %while.29 = (s32[]{:T(128)}, f32[128,64]{0,1:T(8,128)S(1)}, f32[8,64,64]{2,1,0:T(8,128)S(1)}, f32[8,64,128]{2,1,0:T(8,128)S(1)}, f32[8,64,128]{2,1,0:T(8,128)S(1...) while((s32[]{:T(128)}, f32[128,64]{0,1:T(8,128)S(1)}, ...), condition=%wide.region_7.8_spmd.clone.clone, body=%wide.region_4.7_spmd.clone.clone.sunk | while | flops 19451908 | bytes 799868 | solution.py:55
  262.9 1.4 multiply_reduce_fusion.6
  265.1 1.4 multiply_reduce_fusion.6
  267.3 1.4 multiply_reduce_fusion.6
  269.5 1.4 multiply_reduce_fusion.6
  271.6 1.4 multiply_reduce_fusion.6
  273.8 1.4 multiply_reduce_fusion.6
  276.0 1.4 multiply_reduce_fusion.6
  278.2 1.4 multiply_reduce_fusion.6
  280.8 17.5 %while.28 = (s32[]{:T(128)}, f32[128,64]{0,1:T(8,128)S(1)}, f32[8,64,64]{2,1,0:T(8,128)S(1)}, f32[8,64,128]{2,1,0:T(8,128)S(1)}, f32[8,64,128]{2,1,0:T(8,128)S(1...) while((s32[]{:T(128)}, f32[128,64]{0,1:T(8,128)S(1)}, ...), condition=%wide.region_3.4_spmd.clone.clone, body=%wide.region_0.3_spmd.clone.clone.sunk | while | flops 19451908 | bytes 799868 | solution.py:55
  280.9 1.4 multiply_reduce_fusion.5
  283.1 1.4 multiply_reduce_fusion.5
  285.3 1.4 multiply_reduce_fusion.5
  287.5 1.4 multiply_reduce_fusion.5
  289.7 1.4 multiply_reduce_fusion.5
  291.8 1.4 multiply_reduce_fusion.5
  294.0 1.4 multiply_reduce_fusion.5
  296.2 1.4 multiply_reduce_fusion.5
  299.4 0.7 reduce.4
  300.2 0.8 reshape.266
  301.0 5.9 %all-to-all-start.4 = ((bf16[8,2,2048]{2,1,0:T(2,128)(2,1)}), bf16[8,2,2048]{2,1,0:T(2,128)(2,1)S(1)}, u32[]{:S(2)}, u32[]{:S(2)}) async-start(bf16[8,2,2048]{2,1,0:T(2,128)(2,1)} %reshape.266), calls=%async_computation.4 | async-start | bytes 131072 | tf_op jit(solution)/shard_map/all_to_all | solution.py:130
  306.9 6.9 %all-to-all-done.4 = bf16[8,2,2048]{2,1,0:T(2,128)(2,1)S(1)} async-done(((bf16[8,2,2048]{2,1,0:T(2,128)(2,1)}), bf16[8,2,2048]{2,1,0:T(2,128)(2,1)S(1)}, u32[]{:S(2)}, u32[]{:S(2)}) %all-to-all-start.4) | async-done | bytes 65568 | tf_op jit(solution)/shard_map/all_to_all | solution.py:130
  314.7 29.9 %all-gather.17.cloned.1.call-done = bf16[512,1024]{0,1:T(8,128)(2,1)} async-done(((bf16[512,32]{0,1:T(8,128)(2,1)}), bf16[512,1024]{0,1:T(8,128)(2,1)}) %all-gather.17.cloned.1.call-update) | async-done | bytes 1048592 | tf_op jit(solution)/shard_map/all_gather | solution.py:18
  344.8 3.0 fusion.50
  (197 shorter events, 17.0 us)
Async XLA Ops:
  6.5 60.0 %copy-start = (bf16[1,64,1024]{2,1,0:T(8,128)(2,1)S(1)}, bf16[1,64,1024]{2,1,0:T(8,128)(2,1)}, u32[]{:S(2)}) copy-start(bf16[1,64,1024]{2,1,0:T(8,128)(2,1)} %param.14) | copy-start | bytes 393220
  6.5 60.0 %all-gather.13.cloned.1.call-start = ((), (), s32[]{:S(2)}) async-start(), calls=%async_computation.8 | async-start | bytes 1081344 | tf_op jit(solution)/shard_map/all_gather | solution.py:91
  7.3 114.8 %all-gather.9.cloned.1.call-start = ((), (), s32[]{:S(2)}) async-start(), calls=%async_computation.6 | async-start | bytes 1081344 | tf_op jit(solution)/shard_map/all_gather | solution.py:92
  8.0 169.5 %all-gather.11.cloned.1.call-start = ((), (), s32[]{:S(2)}) async-start(), calls=%async_computation.7 | async-start | bytes 1081344 | tf_op jit(solution)/shard_map/all_gather | solution.py:89
  8.7 224.1 %all-gather.7.cloned.1.call-start = ((), (), s32[]{:S(2)}) async-start(), calls=%async_computation.5 | async-start | bytes 1081344 | tf_op jit(solution)/shard_map/all_gather | solution.py:90
  9.3 305.4 %all-gather.15.cloned.1.call-start = ((), (), s32[]{:S(2)}) async-start(), calls=%async_computation.9 | async-start | bytes 1081344 | tf_op jit(solution)/shard_map/all_gather | solution.py:93
  9.9 334.8 %all-gather.17.cloned.1.call-start = ((), (), s32[]{:S(2)}) async-start(), calls=%async_computation.10 | async-start | bytes 1081344 | tf_op jit(solution)/shard_map/all_gather | solution.py:18
  124.7 109.9 %all-to-all-start.1 = ((bf16[8,2,2048]{2,1,0:T(2,128)(2,1)}), bf16[8,2,2048]{2,1,0:T(2,128)(2,1)S(1)}, u32[]{:S(2)}, u32[]{:S(2)}) async-start(bf16[8,2,2048]{2,1,0:T(2,128)(2,1)} %reshape.264), calls=%async_computation.1 | async-start | bytes 131072 | tf_op jit(solution)/shard_map/all_to_all | solution.py:117
  235.2 11.9 %all-to-all-start.3 = ((bf16[64,8,128]{2,0,1:T(8,128)(2,1)}), bf16[64,8,128]{2,0,1:T(8,128)(2,1)S(1)}, u32[]{:S(2)}, u32[]{:S(2)}) async-start(bf16[64,8,128]{2,0,1:T(8,128)(2,1)} %bitcast.17), calls=%async_computation.3 | async-start | bytes 262144 | tf_op jit(solution)/shard_map/all_to_all | solution.py:114
  247.8 10.7 %all-to-all-start.2 = ((bf16[64,8,128]{2,0,1:T(8,128)(2,1)}), bf16[64,8,128]{2,0,1:T(8,128)(2,1)S(1)}, u32[]{:S(2)}, u32[]{:S(2)}) async-start(bf16[64,8,128]{2,0,1:T(8,128)(2,1)} %bitcast.10), calls=%async_computation.2 | async-start | bytes 262144 | tf_op jit(solution)/shard_map/all_to_all | solution.py:108
  259.1 21.2 %all-to-all-start = ((bf16[64,8,128]{2,0,1:T(8,128)(2,1)}), bf16[64,8,128]{2,0,1:T(8,128)(2,1)S(1)}, u32[]{:S(2)}, u32[]{:S(2)}) async-start(bf16[64,8,128]{2,0,1:T(8,128)(2,1)} %bitcast.1), calls=%async_computation | async-start | bytes 262144 | tf_op jit(solution)/shard_map/all_to_all | solution.py:111
  298.2 8.7 %copy-start.1 = (f32[128]{0:T(128)S(1)}, f32[128]{0:T(128)}, u32[]{:S(2)}) copy-start(f32[128]{0:T(128)} %param.23) | copy-start | bytes 1540
  301.0 12.8 %all-to-all-start.4 = ((bf16[8,2,2048]{2,1,0:T(2,128)(2,1)}), bf16[8,2,2048]{2,1,0:T(2,128)(2,1)S(1)}, u32[]{:S(2)}, u32[]{:S(2)}) async-start(bf16[8,2,2048]{2,1,0:T(2,128)(2,1)} %reshape.266), calls=%async_computation.4 | async-start | bytes 131072 | tf_op jit(solution)/shard_map/all_to_all | solution.py:130
Sparse Core Ops, SparseCore 0:
  10.2 56.3 all-gather.12
  69.4 52.5 all-gather.8
  124.9 52.5 all-gather.10
  180.2 52.5 all-gather.6
  235.6 53.3 all-gather.14
  291.7 52.8 all-gather.16
where the time goes:
time: 355 us
  waiting for transfers between devices  265 us (75%)
  other arithmetic  26.9 us (8%)
  starting transfers between devices  21.8 us (6%)
  matrix products  19.3 us (5%)
  between operations  13.8 us (4%)
  local copies, waits for them, and re-layouts  6.91 us (2%)
    all_gather x1, waiting for transfers between devices, body(): lax.all_gather(w_backward, ('sp', 'dp'), axis=1, tiled=True)  54.5 us
    all_gather x1, waiting for transfers between devices, body(): lax.all_gather(w_input, ('sp', 'dp'), axis=1, tiled=True)  53.8 us
    all_gather x1, waiting for transfers between devices, body(): lax.all_gather(w_forward, ('sp', 'dp'), axis=1, tiled=True)  53.6 us
    all_gather x1, waiting for transfers between devices, body(): lax.all_gather(w_query, ('sp', 'dp'), axis=1, tiled=True)  48.4 us
    all_gather x1, waiting for transfers between devices, gathered_then(): everything = lax.all_gather(share, axis, axis=dim, tiled=True)  29.9 us
    reduce_sum x16, other arithmetic, advance(): jnp.sum(query_part[:, None, :] * key_part[None, :, :] * decay_table, axis=2)  21.8 us
  transfers between devices with their start and end apart: 11, of which 8 were waited for; matrix products, arithmetic and copies ran while one was open for 14% of the time, Pallas kernels for 0%

commit v1 on v0

--- a/solution.py
+++ b/solution.py
@@ -2,6 +2,7 @@
 import jax.numpy as jnp
 from jax import lax
 from jax.sharding import PartitionSpec as P
+from jax.lax import all_to_all, axis_size
 
 HEADS = 4
 HEAD_DIM = 128
@@ -86,7 +87,9 @@
     block_width = HEAD_DIM // per_head_groups
     head_index = lax.axis_index("sp") // per_head_groups
     full_query, full_forward, full_backward, full_input, full_gate = (
-        lax.all_gather(w_query, ("sp", "dp"), axis=1, tiled=True),
+        jnp.concatenate(
+            all_to_all(jnp.stack(axis_size(("sp", "dp")) * [w_query]), ("sp", "dp"), 0, 0), axis=1
+        ),
         lax.all_gather(w_forward, ("sp", "dp"), axis=1, tiled=True),
         lax.all_gather(w_backward, ("sp", "dp"), axis=1, tiled=True),
         lax.all_gather(w_input, ("sp", "dp"), axis=1, tiled=True),

time: 355 us -> 302 us (0.85)
  waiting for transfers between devices: 265 us -> 207 us
  starting transfers between devices: 21.8 us -> 25.5 us
    all_gather x1 -> x0, waiting for transfers between devices: 48.4 us -> none  [body(): lax.all_gather(w_query, ('sp', 'dp'), axis=1, tiled=True)]
    all_gather x1, waiting for transfers between devices: 29.9 us -> 14.8 us  [gathered_then(): everything = lax.all_gather(share, axis, axis=dim, tiled=True)]
    all_to_all x0 -> x1, starting transfers between devices: none -> 7.33 us  [body(): all_to_all(jnp.stack(axis_size(('sp', 'dp')) * [w_query]), ('sp', 'dp'),...]
    all_to_all x1, waiting for transfers between devices: 0.01 us -> 7.11 us  [body(): lax.all_to_all(as_sent(by_head(project(full_forward))), 'sp', split_axis=...]
    all_to_all x1, waiting for transfers between devices: 0.01 us -> 6.44 us  [body(): lax.all_to_all(as_sent(by_group(project(full_input))), 'sp', split_axis=1...]
    all_gather x1, waiting for transfers between devices: 54.5 us -> 48.4 us  [body(): lax.all_gather(w_backward, ('sp', 'dp'), axis=1, tiled=True)]
  transfers between devices with their start and end apart: 11 -> 11, of which waited for: 8 -> 9; matrix products, arithmetic and copies ran while one was open for 14% -> 17% of each run, Pallas kernels for 0% -> 0%
where the time goes in v1:
time: 302 us; the launch traced here: 301 us
  waiting for transfers between devices  207 us (69%)
  other arithmetic  26.9 us (9%)
  starting transfers between devices  25.5 us (8%)
  matrix products  18.1 us (6%)
  between operations  13.5 us (4%)
  local copies, waits for them, and re-layouts  8.84 us (3%)
    all_gather x1, waiting for transfers between devices, body(): lax.all_gather(w_input, ('sp', 'dp'), axis=1, tiled=True)  53.8 us
    all_gather x1, waiting for transfers between devices, body(): lax.all_gather(w_forward, ('sp', 'dp'), axis=1, tiled=True)  52.9 us
    all_gather x1, waiting for transfers between devices, body(): lax.all_gather(w_backward, ('sp', 'dp'), axis=1, tiled=True)  48.4 us
    reduce_sum x16, other arithmetic, advance(): jnp.sum(query_part[:, None, :] * key_part[None, :, :] * decay_table, axis=2)  21.8 us
    all_gather x1, waiting for transfers between devices, gathered_then(): everything = lax.all_gather(share, axis, axis=dim, tiled=True)  14.8 us
    all_to_all x1, starting transfers between devices, body(): all_to_all(jnp.stack(axis_size(('sp', 'dp')) * [w_query]), ('sp', 'dp'),...  7.33 us
    all_to_all x1, waiting for transfers between devices, body(): lax.all_to_all(as_sent(by_head(project(full_forward))), 'sp', split_axis=...  7.11 us
    all_to_all x1, waiting for transfers between devices, body(): lax.all_to_all(as_sent(by_head(project(full_backward))), 'sp', split_axis...  6.95 us
  transfers between devices with their start and end apart: 11, of which 9 were waited for; matrix products, arithmetic and copies ran while one was open for 17% of the time, Pallas kernels for 0%

profile of v1, /device:TPU:0, one launch (start us, length us, event | category | flops | bytes accessed | tf_op | source)
XLA Modules:
  0.0 301.4 jit_solution(14765545155925876553)
XLA Ops:
  6.5 0.7 all-gather.10.cloned.1.call-update
  7.3 0.7 all-gather.8.cloned.1.call-update
  8.1 0.7 all-gather.6.cloned.1.call-update
  9.3 1.9 stack.2
  11.2 7.3 %all-to-all-start.2 = ((bf16[32,1024,16]{1,2,0:T(8,128)(2,1)}), bf16[32,1024,16]{1,2,0:T(8,128)(2,1)S(1)}, u32[]{:S(2)}, u32[]{:S(2)}) async-start(bf16[32,1024,16]{1,2,0:T(8,128)(2,1)} %stack.2), calls=%async_computation.2 | async-start | bytes 2097152 | tf_op jit(solution)/shard_map/all_to_all | solution.py:91
  19.2 0.8 negate_log-plus-one_fusion
  19.9 0.8 negate_log-plus-one_fusion.1
  20.7 48.4 %all-gather.10.cloned.1.call-done = bf16[1024,512]{0,1:T(8,128)(2,1)} async-done(((bf16[1024,16]{0,1:T(8,128)(2,1)}), bf16[1024,512]{0,1:T(8,128)(2,1)}) %all-gather.10.cloned.1.call-update) | async-done | bytes 1048592 | tf_op jit(solution)/shard_map/all_gather | solution.py:94
  69.2 1.7 fusion.54
  70.8 53.8 %all-gather.8.cloned.1.call-done = bf16[1024,512]{0,1:T(8,128)(2,1)} async-done(((bf16[1024,16]{0,1:T(8,128)(2,1)}), bf16[1024,512]{0,1:T(8,128)(2,1)}) %all-gather.8.cloned.1.call-update) | async-done | bytes 1048592 | tf_op jit(solution)/shard_map/all_gather | solution.py:95
  124.6 1.7 convolution_convert_fusion.4
  126.5 0.8 reshape.274
  127.2 52.9 %all-gather.6.cloned.1.call-done = bf16[1024,512]{0,1:T(8,128)(2,1)} async-done(((bf16[1024,16]{0,1:T(8,128)(2,1)}), bf16[1024,512]{0,1:T(8,128)(2,1)}) %all-gather.6.cloned.1.call-update) | async-done | bytes 1048592 | tf_op jit(solution)/shard_map/all_gather | solution.py:93
  180.1 1.7 fusion.52
  181.8 4.5 %all-to-all-start.1 = ((bf16[8,2,2048]{2,1,0:T(2,128)(2,1)}), bf16[8,2,2048]{2,1,0:T(2,128)(2,1)S(1)}, u32[]{:S(2)}, u32[]{:S(2)}) async-start(bf16[8,2,2048]{2,1,0:T(2,128)(2,1)} %reshape.274), calls=%async_computation.1 | async-start | bytes 131072 | tf_op jit(solution)/shard_map/all_to_all | solution.py:120
  186.8 6.4 %all-to-all-done.1 = bf16[8,2,2048]{2,1,0:T(2,128)(2,1)S(1)} async-done(((bf16[8,2,2048]{2,1,0:T(2,128)(2,1)}), bf16[8,2,2048]{2,1,0:T(2,128)(2,1)S(1)}, u32[]{:S(2)}, u32[]{:S(2)}) %all-to-all-start.1) | async-done | bytes 65568 | tf_op jit(solution)/shard_map/all_to_all | solution.py:120
  193.2 0.7 broadcast_in_dim.94
  193.9 3.4 %all-to-all-start.4 = ((bf16[64,8,128]{2,0,1:T(8,128)(2,1)}), bf16[64,8,128]{2,0,1:T(8,128)(2,1)S(1)}, u32[]{:S(2)}, u32[]{:S(2)}) async-start(bf16[64,8,128]{2,0,1:T(8,128)(2,1)} %bitcast.19), calls=%async_computation.4 | async-start | bytes 262144 | tf_op jit(solution)/shard_map/all_to_all | solution.py:117
  197.6 6.9 %all-to-all-done.4 = bf16[64,8,128]{2,0,1:T(8,128)(2,1)S(1)} async-done(((bf16[64,8,128]{2,0,1:T(8,128)(2,1)}), bf16[64,8,128]{2,0,1:T(8,128)(2,1)S(1)}, u32[]{:S(2)}, u32[]{:S(2)}) %all-to-all-start.4) | async-done | bytes 131104 | tf_op jit(solution)/shard_map/all_to_all | solution.py:117
  204.6 0.7 broadcast_in_dim.90
  205.2 3.4 %all-to-all-start = ((bf16[64,8,128]{2,0,1:T(8,128)(2,1)}), bf16[64,8,128]{2,0,1:T(8,128)(2,1)S(1)}, u32[]{:S(2)}, u32[]{:S(2)}) async-start(bf16[64,8,128]{2,0,1:T(8,128)(2,1)} %bitcast.1), calls=%async_computation | async-start | bytes 262144 | tf_op jit(solution)/shard_map/all_to_all | solution.py:114
  209.1 7.1 %all-to-all-done = bf16[64,8,128]{2,0,1:T(8,128)(2,1)S(1)} async-done(((bf16[64,8,128]{2,0,1:T(8,128)(2,1)}), bf16[64,8,128]{2,0,1:T(8,128)(2,1)S(1)}, u32[]{:S(2)}, u32[]{:S(2)}) %all-to-all-start) | async-done | bytes 131104 | tf_op jit(solution)/shard_map/all_to_all | solution.py:114
  216.2 0.7 broadcast_in_dim.92
  216.9 3.4 %all-to-all-start.3 = ((bf16[64,8,128]{2,0,1:T(8,128)(2,1)}), bf16[64,8,128]{2,0,1:T(8,128)(2,1)S(1)}, u32[]{:S(2)}, u32[]{:S(2)}) async-start(bf16[64,8,128]{2,0,1:T(8,128)(2,1)} %bitcast.12), calls=%async_computation.3 | async-start | bytes 262144 | tf_op jit(solution)/shard_map/all_to_all | solution.py:111
  220.8 6.9 %all-to-all-done.3 = bf16[64,8,128]{2,0,1:T(8,128)(2,1)S(1)} async-done(((bf16[64,8,128]{2,0,1:T(8,128)(2,1)}), bf16[64,8,128]{2,0,1:T(8,128)(2,1)S(1)}, u32[]{:S(2)}, u32[]{:S(2)}) %all-to-all-start.3) | async-done | bytes 131104 | tf_op jit(solution)/shard_map/all_to_all | solution.py:111
  227.9 17.5 %while.29 = (s32[]{:T(128)}, f32[128,64]{0,1:T(8,128)S(1)}, f32[8,64,64]{2,1,0:T(8,128)S(1)}, f32[8,64,128]{2,1,0:T(8,128)S(1)}, f32[8,64,128]{2,1,0:T(8,128)S(1...) while((s32[]{:T(128)}, f32[128,64]{0,1:T(8,128)S(1)}, ...), condition=%wide.region_7.8_spmd.clone.clone, body=%wide.region_4.7_spmd.clone.clone.sunk | while | flops 19451908 | bytes 799868 | solution.py:56
  228.1 1.4 multiply_reduce_fusion.6
  230.3 1.4 multiply_reduce_fusion.6
  232.4 1.4 multiply_reduce_fusion.6
  234.6 1.4 multiply_reduce_fusion.6
  236.8 1.4 multiply_reduce_fusion.6
  239.0 1.4 multiply_reduce_fusion.6
  241.2 1.4 multiply_reduce_fusion.6
  243.4 1.4 multiply_reduce_fusion.6
  245.5 17.5 %while.28 = (s32[]{:T(128)}, f32[128,64]{0,1:T(8,128)S(1)}, f32[8,64,64]{2,1,0:T(8,128)S(1)}, f32[8,64,128]{2,1,0:T(8,128)S(1)}, f32[8,64,128]{2,1,0:T(8,128)S(1...) while((s32[]{:T(128)}, f32[128,64]{0,1:T(8,128)S(1)}, ...), condition=%wide.region_3.4_spmd.clone.clone, body=%wide.region_0.3_spmd.clone.clone.sunk | while | flops 19451908 | bytes 799868 | solution.py:56
  245.7 1.4 multiply_reduce_fusion.5
  247.9 1.4 multiply_reduce_fusion.5
  250.0 1.4 multiply_reduce_fusion.5
  252.2 1.4 multiply_reduce_fusion.5
  254.4 1.4 multiply_reduce_fusion.5
  256.6 1.4 multiply_reduce_fusion.5
  258.8 1.4 multiply_reduce_fusion.5
  261.0 1.4 multiply_reduce_fusion.5
  264.9 0.8 reshape.276
  265.7 3.4 %all-to-all-start.5 = ((bf16[8,2,2048]{2,1,0:T(2,128)(2,1)}), bf16[8,2,2048]{2,1,0:T(2,128)(2,1)S(1)}, u32[]{:S(2)}, u32[]{:S(2)}) async-start(bf16[8,2,2048]{2,1,0:T(2,128)(2,1)} %reshape.276), calls=%async_computation.5 | async-start | bytes 131072 | tf_op jit(solution)/shard_map/all_to_all | solution.py:133
  269.1 6.8 %all-to-all-done.5 = bf16[8,2,2048]{2,1,0:T(2,128)(2,1)S(1)} async-done(((bf16[8,2,2048]{2,1,0:T(2,128)(2,1)}), bf16[8,2,2048]{2,1,0:T(2,128)(2,1)S(1)}, u32[]{:S(2)}, u32[]{:S(2)}) %all-to-all-start.5) | async-done | bytes 65568 | tf_op jit(solution)/shard_map/all_to_all | solution.py:133
  276.9 14.8 %all-gather.14.cloned.1.call-done = bf16[512,1024]{0,1:T(8,128)(2,1)} async-done(((bf16[512,32]{0,1:T(8,128)(2,1)}), bf16[512,1024]{0,1:T(8,128)(2,1)}) %all-gather.14.cloned.1.call-update) | async-done | bytes 1048592 | tf_op jit(solution)/shard_map/all_gather | solution.py:19
  291.8 3.0 %fusion.50 = bf16[1,64,1024]{2,1,0:T(8,128)(2,1)} fusion(bf16[512,1024]{0,1:T(8,128)(2,1)} %all-gather.14.cloned.1.call-done, f32[64,512]{1,0:T(8,128)S(1)} %reshape.268, f32[8,8,4,128]{3,2,1,0:T(4,128)S(1)} %bitcast.290, bf16[1024,512]{0,1:T(8,128)(2,1)} %all-gather.12.cloned.1.call-done, bf16[1,64,1024]{2,1,0:T(8,128)(2,1)S(1)} %copy-done, ...), kind=kOutput, calls=%fused_computation.65 | convolution fusion | flops 134610944 | bytes 2623488 | tf_op jit(solution)/shard_map/dot_general | solution.py:146
  (197 shorter events, 18.1 us)
Async XLA Ops:
  6.5 62.6 %copy-start = (bf16[1,64,1024]{2,1,0:T(8,128)(2,1)S(1)}, bf16[1,64,1024]{2,1,0:T(8,128)(2,1)}, u32[]{:S(2)}) copy-start(bf16[1,64,1024]{2,1,0:T(8,128)(2,1)} %param.14) | copy-start | bytes 393220
  6.5 62.6 %all-gather.10.cloned.1.call-start = ((), (), s32[]{:S(2)}) async-start(), calls=%async_computation.8 | async-start | bytes 1081344 | tf_op jit(solution)/shard_map/all_gather | solution.py:94
  7.3 117.4 %all-gather.8.cloned.1.call-start = ((), (), s32[]{:S(2)}) async-start(), calls=%async_computation.7 | async-start | bytes 1081344 | tf_op jit(solution)/shard_map/all_gather | solution.py:95
  8.0 172.1 %all-gather.6.cloned.1.call-start = ((), (), s32[]{:S(2)}) async-start(), calls=%async_computation.6 | async-start | bytes 1081344 | tf_op jit(solution)/shard_map/all_gather | solution.py:93
  8.7 268.1 %all-gather.12.cloned.1.call-start = ((), (), s32[]{:S(2)}) async-start(), calls=%async_computation.9 | async-start | bytes 1081344 | tf_op jit(solution)/shard_map/all_gather | solution.py:96
  11.2 170.6 %all-to-all-start.2 = ((bf16[32,1024,16]{1,2,0:T(8,128)(2,1)}), bf16[32,1024,16]{1,2,0:T(8,128)(2,1)S(1)}, u32[]{:S(2)}, u32[]{:S(2)}) async-start(bf16[32,1024,16]{1,2,0:T(8,128)(2,1)} %stack.2), calls=%async_computation.2 | async-start | bytes 2097152 | tf_op jit(solution)/shard_map/all_to_all | solution.py:91
  18.5 273.1 %all-gather.14.cloned.1.call-start = ((), (), s32[]{:S(2)}) async-start(), calls=%async_computation.10 | async-start | bytes 1081344 | tf_op jit(solution)/shard_map/all_gather | solution.py:19
  181.8 11.4 %all-to-all-start.1 = ((bf16[8,2,2048]{2,1,0:T(2,128)(2,1)}), bf16[8,2,2048]{2,1,0:T(2,128)(2,1)S(1)}, u32[]{:S(2)}, u32[]{:S(2)}) async-start(bf16[8,2,2048]{2,1,0:T(2,128)(2,1)} %reshape.274), calls=%async_computation.1 | async-start | bytes 131072 | tf_op jit(solution)/shard_map/all_to_all | solution.py:120
  193.9 10.7 %all-to-all-start.4 = ((bf16[64,8,128]{2,0,1:T(8,128)(2,1)}), bf16[64,8,128]{2,0,1:T(8,128)(2,1)S(1)}, u32[]{:S(2)}, u32[]{:S(2)}) async-start(bf16[64,8,128]{2,0,1:T(8,128)(2,1)} %bitcast.19), calls=%async_computation.4 | async-start | bytes 262144 | tf_op jit(solution)/shard_map/all_to_all | solution.py:117
  205.2 11.0 %all-to-all-start = ((bf16[64,8,128]{2,0,1:T(8,128)(2,1)}), bf16[64,8,128]{2,0,1:T(8,128)(2,1)S(1)}, u32[]{:S(2)}, u32[]{:S(2)}) async-start(bf16[64,8,128]{2,0,1:T(8,128)(2,1)} %bitcast.1), calls=%async_computation | async-start | bytes 262144 | tf_op jit(solution)/shard_map/all_to_all | solution.py:114
  216.9 10.8 %all-to-all-start.3 = ((bf16[64,8,128]{2,0,1:T(8,128)(2,1)}), bf16[64,8,128]{2,0,1:T(8,128)(2,1)S(1)}, u32[]{:S(2)}, u32[]{:S(2)}) async-start(bf16[64,8,128]{2,0,1:T(8,128)(2,1)} %bitcast.12), calls=%async_computation.3 | async-start | bytes 262144 | tf_op jit(solution)/shard_map/all_to_all | solution.py:111
  263.0 6.1 %copy-start.1 = (f32[128]{0:T(128)S(1)}, f32[128]{0:T(128)}, u32[]{:S(2)}) copy-start(f32[128]{0:T(128)} %param.23) | copy-start | bytes 1540
  265.7 10.2 %all-to-all-start.5 = ((bf16[8,2,2048]{2,1,0:T(2,128)(2,1)}), bf16[8,2,2048]{2,1,0:T(2,128)(2,1)S(1)}, u32[]{:S(2)}, u32[]{:S(2)}) async-start(bf16[8,2,2048]{2,1,0:T(2,128)(2,1)} %reshape.276), calls=%async_computation.5 | async-start | bytes 131072 | tf_op jit(solution)/shard_map/all_to_all | solution.py:133
Sparse Core Ops, SparseCore 0:
  10.2 58.9 all-gather.9
  72.0 52.5 all-gather.7
  127.5 52.5 all-gather.5
  182.8 52.9 all-gather.11
  238.6 53.0 all-gather.13
